TPU v7x, 32 devices: a whole 2x2x4 slice. The times are simulated.
32 devices in a mesh: grp: 2 (over y), sp: 4 (over z), tp: 4 (over x, core).
Axes of the slice: x: 2, y: 2, z: 4, core: 2. Of those that a mesh axis runs over, the one named last changes fastest.
Arguments:
- tokens: bfloat16 [2048, 8, 2048], P('sp', 'grp'), parts along dimension 1, may hold values from -48 to 48
- query_weight: bfloat16 [2048, 1024], P(None, 'tp'), may hold values from -2 to 2
- key_weight: bfloat16 [2048, 1024], P(None, 'tp'), may hold values from -2 to 2
- value_weight: bfloat16 [2048, 1024], P(None, 'tp'), may hold values from -3 to 3
- mix_gain: float32 [1024], P('tp'), may hold values from 0.1 to 1.9
- out_weight: bfloat16 [1024, 2048], P('tp'), may hold values from -0.1875 to 0.1875
Outputs:
- mixed: bfloat16 [2048, 8, 2048], P(('sp', 'tp'), 'grp'), parts along dimension 1
There are 2 independent parts, one for each index of `grp`. A program takes and returns all parts, laid end to end along the dimension named above; an argument that names none is the same for every part. Nothing has to cross between parts.
All inputs are finite; a program needn't handle non-finite values.
Results may differ from a plain program's by a relative error of at most 0.02.
Values may be sent and summed in bfloat16 or wider, within the bound.
A program may use at most 128 MiB of HBM per device.

v0:
```python
import functools

import jax
import jax.numpy as jnp
from jax import lax
from jax.experimental import pallas as pl
from jax.experimental.pallas import tpu as pltpu
from jax.sharding import PartitionSpec as P

HEAD_DIM = 64
PATTERNS = ((128, 1), (512, 4), (2048, 16))
REACH = 128
CLASSES = 16
EPSILON = 1e-06
NEGATIVE = -1e30
GROUPS = 2


def attend_kernel(q_ref, k_ref, v_ref, o_ref, out_sc, top_sc, sum_sc, near_bias, mid_bias, far_bias):
    chunks, _, per_class, width = q_ref.shape
    heads = width // HEAD_DIM
    tile = 16
    near_rows = CLASSES * tile
    mid_rows = 4 * per_class
    span = REACH // per_class
    far_tiles = chunks // span

    def bias_of(diff, window, live):
        return jnp.where((diff >= 0) & (diff <= window) & live, 0.0, NEGATIVE).astype(jnp.float32)

    row = lax.broadcasted_iota(jnp.int32, near_bias.shape[1:], 0)
    col = lax.broadcasted_iota(jnp.int32, near_bias.shape[1:], 1)
    diff = (row % tile - col % tile) * 16 + row // tile - (col % near_rows) // tile
    diff = diff + jnp.where(col < near_rows, near_rows, 0)
    near_bias[0] = bias_of(diff, PATTERNS[0][0], col >= near_rows)
    near_bias[1] = bias_of(diff, PATTERNS[0][0], col >= 0)
    row = lax.broadcasted_iota(jnp.int32, mid_bias.shape[1:], 0)
    col = lax.broadcasted_iota(jnp.int32, mid_bias.shape[1:], 1)
    diff = (row % per_class - col % per_class) * 16
    diff = diff + 4 * (row // per_class - (col % mid_rows) // per_class)
    diff = diff + jnp.where(col < mid_rows, CLASSES * per_class, 0)
    mid_bias[0] = bias_of(diff, PATTERNS[1][0], col >= mid_rows)
    mid_bias[1] = bias_of(diff, PATTERNS[1][0], col >= 0)
    row = lax.broadcasted_iota(jnp.int32, far_bias.shape, 0)
    col = lax.broadcasted_iota(jnp.int32, far_bias.shape, 1)
    far_bias[...] = bias_of(row + REACH - col, REACH, col >= 0)

    lane = lax.broadcasted_iota(jnp.int32, (1, width), 1) // HEAD_DIM
    picks = [jnp.where(lane == h, HEAD_DIM ** -0.5, 0.0).astype(jnp.bfloat16) for h in range(heads)]

    def attend(queries, keys, values, bias):
        outs, tops, sums = [], [], []
        for h in range(heads):
            scores = lax.dot_general(
                queries * picks[h], keys, (((1,), (1,)), ((), ())), preferred_element_type=jnp.float32
            ) + bias
            top = jnp.max(scores, axis=1, keepdims=True)
            raised = jnp.exp(scores - top)
            total = jnp.sum(raised, axis=1, keepdims=True)
            outs.append(jnp.dot(raised.astype(jnp.bfloat16), values, preferred_element_type=jnp.float32))
            tops.append(jnp.broadcast_to(top, outs[-1].shape))
            sums.append(jnp.broadcast_to(total, outs[-1].shape))

        def join(parts):
            whole = parts[0]
            for h in range(1, heads):
                whole = jnp.where(lane == h, parts[h], whole)
            return whole

        return join(outs), join(tops), join(sums)

    def merge_rows(ref, *index):
        block = ref[index]
        return block.reshape(-1, width)

    @pl.loop(0, chunks)
    def near_and_mid(z):
        before = jnp.maximum(z - 1, 0)
        first = jnp.minimum(z, 1)
        for u in range(per_class // tile):
            rows = slice(u * tile, (u + 1) * tile)
            back, back_rows, kind = (before, slice(per_class - tile, per_class), first)
            if u > 0:
                back, back_rows, kind = (z, slice((u - 1) * tile, u * tile), 1)
            queries = q_ref[z, :, rows, :].reshape(near_rows, width)
            keys, values = (
                jnp.concatenate(
                    [
                        ref[back, :, back_rows, :].reshape(near_rows, width),
                        ref[z, :, rows, :].reshape(near_rows, width),
                    ],
                    axis=0,
                )
                for ref in (k_ref, v_ref)
            )
            for ref, part in zip((out_sc, top_sc, sum_sc), attend(queries, keys, values, near_bias[kind])):
                ref[0, z, :, rows, :] = part.reshape(CLASSES, tile, width)
        for r in range(4):
            classes = range(r, CLASSES, 4)
            queries = jnp.concatenate([q_ref[z, c] for c in classes], axis=0)
            keys, values = (
                jnp.concatenate([ref[y, c] for y in (before, z) for c in classes], axis=0)
                for ref in (k_ref, v_ref)
            )
            for ref, part in zip((out_sc, top_sc, sum_sc), attend(queries, keys, values, mid_bias[first])):
                for m, c in enumerate(classes):
                    ref[1, z, c] = part[m * per_class : (m + 1) * per_class]

    @pl.loop(0, CLASSES // 4)
    def far(quad):
        for inner in range(4):
            c = quad * 4 + inner
            for n in range(far_tiles):
                here = slice(n * span, (n + 1) * span)
                reach = slice(max(n - 1, 0) * span, (n + 1) * span)
                queries = q_ref[here, c].reshape(REACH, width)
                keys, values = (ref[reach, c].reshape(-1, width) for ref in (k_ref, v_ref))
                bias = far_bias[...] if n > 0 else far_bias[:, REACH:]
                for ref, part in zip((out_sc, top_sc, sum_sc), attend(queries, keys, values, bias)):
                    ref[2, here, c] = part.reshape(span, per_class, width)

    @pl.loop(0, chunks)
    def mix(z):
        tops = [top_sc[p, z] for p in range(3)]
        highest = jnp.maximum(jnp.maximum(tops[0], tops[1]), tops[2])
        lifts = [jnp.exp(top - highest) for top in tops]
        total = sum(lift * sum_sc[p, z] for p, lift in enumerate(lifts))
        result = sum(lift * out_sc[p, z] for p, lift in enumerate(lifts))
        o_ref[z] = (result / total).astype(o_ref.dtype)


def attend_all(moved, width):
    chunks, batches, _, per_class, triple = moved.shape
    channels = triple // 3
    pairs = channels // width
    if width % 128 == 0:
        operands = (moved, moved, moved)
        starts = (0, pairs, 2 * pairs)
    else:
        operands = tuple(moved[..., i * channels : (i + 1) * channels] for i in range(3))
        starts = (0, 0, 0)
    block = (chunks, None, CLASSES, per_class, width)
    tokens = chunks * CLASSES * per_class
    return pl.pallas_call(
        attend_kernel,
        grid=(batches, pairs),
        in_specs=[
            pl.BlockSpec(block, functools.partial(lambda s, b, i: (0, b, 0, 0, s + i), start)) for start in starts
        ],
        out_specs=pl.BlockSpec(block, lambda b, i: (0, b, 0, 0, i)),
        out_shape=jax.ShapeDtypeStruct((chunks, batches, CLASSES, per_class, channels), jnp.bfloat16),
        scratch_shapes=[pltpu.VMEM((3, chunks, CLASSES, per_class, width), jnp.float32) for _ in range(3)]
        + [
            pltpu.VMEM((2, 256, 512), jnp.float32),
            pltpu.VMEM((2, 4 * per_class, 8 * per_class), jnp.float32),
            pltpu.VMEM((REACH, 2 * REACH), jnp.float32),
        ],
        cost_estimate=pl.CostEstimate(
            flops=tokens * batches * channels * 4 * 900,
            bytes_accessed=tokens * batches * channels * 8,
            transcendentals=tokens * batches * channels // HEAD_DIM * 900,
        ),
    )(*operands)


def body(tokens, query_weight, key_weight, value_weight, mix_gain, out_weight):
    seq_rows, batch_size, features = tokens.shape
    channels = query_weight.shape[1]
    sp_count = lax.axis_size("sp")
    tp_count = lax.axis_size("tp")
    tp_place = lax.axis_index("tp")
    per_class = seq_rows // CLASSES
    head_split = min(max(1, sp_count // batch_size), channels // HEAD_DIM)
    copies = max(1, sp_count // (batch_size * head_split))
    batches = max(1, batch_size // sp_count)
    groups = GROUPS if head_split == 1 else 1

    own = (out_weight.astype(jnp.float32) * mix_gain[:, None]).astype(jnp.bfloat16)
    gathered = [own]
    for step in range(1, tp_count):
        route = [(i, (i + step) % tp_count) for i in range(tp_count)]
        gathered.append(lax.ppermute(own, "tp", route))

    flat = tokens.reshape(per_class, CLASSES, batch_size, features).transpose(2, 1, 0, 3)
    flat = flat.reshape(batch_size * seq_rows, features)
    cut = channels // groups // head_split
    width = min(cut, 2 * HEAD_DIM)
    results = []
    for g in range(groups):
        columns = []
        for s in range(head_split):
            at = (g * head_split + s) * cut
            columns += [w[:, at : at + cut] for w in (query_weight, key_weight, value_weight)]
        product = jnp.dot(flat, jnp.concatenate(columns, axis=1), preferred_element_type=jnp.float32)
        product = product.astype(jnp.bfloat16).reshape(batch_size, seq_rows, head_split, 3 * cut)
        if head_split > 1:
            product = product.transpose(0, 2, 1, 3)
        product = product.reshape(sp_count // copies, batches * seq_rows, 3 * cut)
        if copies > 1:
            product = jnp.repeat(product, copies, axis=0)
        moved = lax.all_to_all(product, "sp", split_axis=0, concat_axis=0, tiled=True)
        moved = moved.reshape(sp_count, batches, CLASSES, per_class, 3 * cut)
        results.append(attend_all(moved, width))

    part = per_class // tp_count
    backs = []
    for result in results:
        back = result.reshape(sp_count, batches, CLASSES, tp_count, part, cut).transpose(0, 3, 1, 2, 4, 5)
        back = back.reshape(sp_count * tp_count, batches * CLASSES * part, cut)
        back = lax.all_to_all(back, ("sp", "tp"), split_axis=0, concat_axis=0, tiled=True)
        back = back.reshape(batch_size // batches, head_split, copies, tp_count, batches, CLASSES, part, cut)[:, :, 0]
        backs.append(back)
    combined = jnp.stack(backs, axis=0).transpose(3, 6, 5, 1, 4, 0, 2, 7)
    rows = part * CLASSES * batch_size
    combined = combined.reshape(tp_count, rows, channels)
    flipped = combined[::-1]
    turned = lax.dynamic_slice_in_dim(
        jnp.concatenate([flipped, flipped], axis=0), tp_count - 1 - tp_place, tp_count, axis=0
    )
    turned = turned.transpose(1, 0, 2).reshape(rows, tp_count * channels)
    wide = turned.astype(jnp.float32)
    row_scale = lax.rsqrt(jnp.mean(wide * wide, axis=-1, keepdims=True) + EPSILON)
    mixed = jnp.dot(turned, jnp.concatenate(gathered, axis=0), preferred_element_type=jnp.float32) * row_scale
    return mixed.astype(jnp.bfloat16).reshape(part * CLASSES, batch_size, out_weight.shape[1])


def solution(mesh):
    in_specs = (
        P("sp", "grp", None),
        P(None, "tp"),
        P(None, "tp"),
        P(None, "tp"),
        P("tp"),
        P("tp", None),
    )
    out_specs = P(("sp", "tp"), "grp", None)
    return jax.shard_map(body, mesh=mesh, in_specs=in_specs, out_specs=out_specs, check_vma=False)
```

profile of v0, /device:TPU:0, one launch (start us, length us, event | category | flops | bytes accessed | tf_op | source)
XLA Modules:
  0.0 208.3 jit_solution(8512876102084646494)
XLA Ops:
  0.0 11.3 %copy.16 = bf16[512,4,2048]{2,0,1:T(8,128)(2,1)} copy(bf16[512,4,2048]{2,1,0:T(4,128)(2,1)} %param.6) | data formatting | bytes 16777216 | tf_op args[0]
  11.3 11.5 %copy.17 = bf16[4,16,32,2048]{3,2,1,0:T(8,128)(2,1)} copy(bf16[4,16,32,2048]{3,1,2,0:T(8,128)(2,1)} %bitcast.33) | data formatting | bytes 16777216 | tf_op jit(solution)/shard_map/transpose | solution.py:184
  22.8 0.9 fusion.30
  23.7 1.3 fusion.28
  25.0 7.1 %fusion.11 = bf16[2048,384]{0,1:T(8,128)(2,1)S(1)} fusion(bf16[2048,2048]{1,0:T(8,128)(2,1)} %bitcast.34, bf16[2048,128]{1,0:T(8,128)(2,1)S(1)} %get-tuple-element.12, bf16[2048,128]{1,0:T(8,128)(2,1)S(1)} %get-tuple-element.13, bf16[2048,128]{1,0:T(8,128)(2,1)S(1)} %get-tuple-element.8), kind=kOutput, calls=%fused_computation.12 | convolution fusion | flops 3226730496 | bytes 11534336 | tf_op jit(solution)/shard_map/dot_general | solution.py:194
  32.2 1.6 copy.26
  33.8 6.4 %all-to-all-start.2 = ((bf16[4,512,384]{2,1,0:T(8,128)(2,1)}), bf16[4,512,384]{2,1,0:T(8,128)(2,1)S(1)}, u32[]{:S(2)}, u32[]{:S(2)}) async-start(bf16[4,512,384]{2,1,0:T(8,128)(2,1)} %bitcast.11), calls=%async_computation.2 | async-start | bytes 3145728 | tf_op jit(solution)/shard_map/all_to_all | solution.py:201
  40.1 7.3 %fusion.10 = bf16[2048,384]{0,1:T(8,128)(2,1)S(1)} fusion(bf16[2048,2048]{1,0:T(8,128)(2,1)} %bitcast.35, bf16[2048,128]{1,0:T(8,128)(2,1)} %get-tuple-element.11, bf16[2048,128]{1,0:T(8,128)(2,1)} %get-tuple-element.14, bf16[2048,128]{1,0:T(8,128)(2,1)} %get-tuple-element.7), kind=kOutput, calls=%fused_computation.11 | convolution fusion | flops 3226730496 | bytes 11534336 | tf_op jit(solution)/shard_map/dot_general | solution.py:194
  47.5 1.6 copy.25
  49.1 28.0 %all-to-all-done.2 = bf16[4,512,384]{2,1,0:T(8,128)(2,1)S(1)} async-done(((bf16[4,512,384]{2,1,0:T(8,128)(2,1)}), bf16[4,512,384]{2,1,0:T(8,128)(2,1)S(1)}, u32[]{:S(2)}, u32[]{:S(2)}) %all-to-all-start.2) | async-done | bytes 1572896 | tf_op jit(solution)/shard_map/all_to_all | solution.py:201
  77.1 3.6 %all-to-all-start = ((bf16[4,512,384]{2,1,0:T(8,128)(2,1)}), bf16[4,512,384]{2,1,0:T(8,128)(2,1)S(1)}, u32[]{:S(2)}, u32[]{:S(2)}) async-start(bf16[4,512,384]{2,1,0:T(8,128)(2,1)} %bitcast.4), calls=%async_computation | async-start | bytes 3145728 | tf_op jit(solution)/shard_map/all_to_all | solution.py:201
  80.6 18.7 %shard_map.65 = bf16[4,1,16,32,128]{4,3,2,1,0:T(8,128)(2,1)} custom-call(bf16[4,1,16,32,384]{4,3,2,1,0:T(8,128)(2,1)} %bitcast.38, bf16[4,1,16,32,384]{4,3,2,1,0:T(8,128)(2,1)} %bitcast.39, bf16[4,1,16,32,384]{4,3,2,1,0:T(8,128)(2,1)} %bitcast.40), custom_call_target="tpu_custom_call" | custom-call | flops 943718400 | bytes 2097152 | tf_op jit(solution)/shard_map/pallas_call | solution.py:144
  99.4 2.0 copy.21
  101.4 15.7 %all-to-all-done = bf16[4,512,384]{2,1,0:T(8,128)(2,1)S(1)} async-done(((bf16[4,512,384]{2,1,0:T(8,128)(2,1)}), bf16[4,512,384]{2,1,0:T(8,128)(2,1)S(1)}, u32[]{:S(2)}, u32[]{:S(2)}) %all-to-all-start) | async-done | bytes 1572896 | tf_op jit(solution)/shard_map/all_to_all | solution.py:201
  117.1 3.8 %all-to-all-start.3 = ((bf16[16,128,128]{2,1,0:T(8,128)(2,1)}), bf16[16,128,128]{2,1,0:T(8,128)(2,1)S(1)}, u32[]{:S(2)}, u32[]{:S(2)}) async-start(bf16[16,128,128]{2,1,0:T(8,128)(2,1)} %bitcast.15), calls=%async_computation.3 | async-start | bytes 1048576 | tf_op jit(solution)/shard_map/all_to_all | solution.py:210
  121.0 18.8 %shard_map.64 = bf16[4,1,16,32,128]{4,3,2,1,0:T(8,128)(2,1)} custom-call(bf16[4,1,16,32,384]{4,3,2,1,0:T(8,128)(2,1)} %bitcast.41, bf16[4,1,16,32,384]{4,3,2,1,0:T(8,128)(2,1)} %bitcast.42, bf16[4,1,16,32,384]{4,3,2,1,0:T(8,128)(2,1)} %bitcast.43), custom_call_target="tpu_custom_call" | custom-call | flops 943718400 | bytes 2097152 | tf_op jit(solution)/shard_map/pallas_call | solution.py:144
  139.8 2.0 copy.19
  141.8 5.9 %all-to-all-start.1 = ((bf16[16,128,128]{2,1,0:T(8,128)(2,1)}), bf16[16,128,128]{2,1,0:T(8,128)(2,1)S(1)}, u32[]{:S(2)}, u32[]{:S(2)}) async-start(bf16[16,128,128]{2,1,0:T(8,128)(2,1)} %bitcast.8), calls=%async_computation.1 | async-start | bytes 1048576 | tf_op jit(solution)/shard_map/all_to_all | solution.py:210
  147.8 1.2 multiply_convert_fusion.1
  149.0 1.6 collective-permute-start.2
  150.6 0.4 collective-permute-start.1
  151.1 1.1 copy.23
  152.2 9.8 %all-to-all-done.1 = bf16[16,128,128]{2,1,0:T(8,128)(2,1)S(1)} async-done(((bf16[16,128,128]{2,1,0:T(8,128)(2,1)}), bf16[16,128,128]{2,1,0:T(8,128)(2,1)S(1)}, u32[]{:S(2)}, u32[]{:S(2)}) %all-to-all-start.1) | async-done | bytes 524320 | tf_op jit(solution)/shard_map/all_to_all | solution.py:210
  162.0 1.1 copy.22
  163.1 2.4 %maximum_bitcast_fusion = bf16[4,8,16,4,1,2,1,128]{7,5,3,2,1,0,6,4:T(2,128)(2,1)S(1)} fusion(bf16[1,4,1,4,1,16,8,128]{7,0,1,5,6,3,2,4:T(2,128)(2,1)S(1)} %copy.23, bf16[1,4,1,4,1,16,8,128]{7,0,1,5,6,3,2,4:T(2,128)(2,1)S(1)} %copy.22), kind=kLoop, calls=%fused_computation.29 | loop fusion | flops 2097152 | bytes 2097152 | tf_op jit(solution)/shard_map/transpose | solution.py:213
  165.6 0.7 reshape.50
  166.3 0.6 multiply_reduce_fusion
  167.0 0.5 copy.24
  167.5 10.5 %collective-permute-done.2 = bf16[256,2048]{1,0:T(8,128)(2,1)} collective-permute-done((bf16[256,2048]{1,0:T(8,128)(2,1)}, bf16[256,2048]{1,0:T(8,128)(2,1)}, u32[]{:S(2)}, u32[]{:S(2)}) %collective-permute-start.2) | collective-permute-done | bytes 1048608 | tf_op jit(solution)/shard_map/ppermute | solution.py:182
  178.0 23.5 %collective-permute-done.1 = bf16[256,2048]{1,0:T(8,128)(2,1)} collective-permute-done((bf16[256,2048]{1,0:T(8,128)(2,1)}, bf16[256,2048]{1,0:T(8,128)(2,1)}, u32[]{:S(2)}, u32[]{:S(2)}) %collective-permute-start.1) | collective-permute-done | bytes 1048608 | tf_op jit(solution)/shard_map/ppermute | solution.py:182
  201.5 4.5 %multiply_convert_fusion = bf16[512,2048]{1,0:T(8,128)(2,1)S(1)} fusion(bf16[512,1024]{0,1:T(8,128)(2,1)S(1)} %bitcast.44, bf16[256,2048]{1,0:T(8,128)(2,1)} %collective-permute-done.2, bf16[256,2048]{1,0:T(8,128)(2,1)} %collective-permute-done.1, bf16[256,2048]{1,0:T(8,128)(2,1)} %collective-permute-done, bf16[256,2048]{1,0:T(8,128)(2,1)} %multiply_convert_fusion.1, ...), kind=kOutput, calls=%fused_computation.8 | convolution fusion | flops 2166358016 | bytes 7342080 | tf_op jit(solution)/shard_map/dot_general | solution.py:223
  206.1 2.2 %reshape.52 = bf16[128,4,2048]{2,1,0:T(4,128)(2,1)} reshape(bf16[512,2048]{1,0:T(8,128)(2,1)S(1)} %multiply_convert_fusion) | data formatting | bytes 4194304 | tf_op jit(solution)/shard_map/reshape | solution.py:224
  (19 shorter events, 0.2 us)
Async XLA Ops:
  11.3 11.5 %copy-start.2 = (bf16[2048,256]{1,0:T(8,128)(2,1)S(1)}, bf16[2048,256]{1,0:T(8,128)(2,1)}, u32[]{:S(2)}) copy-start(bf16[2048,256]{1,0:T(8,128)(2,1)} %param.9) | copy-start | bytes 3145732
  11.3 12.5 %copy-start.4 = (bf16[2048,256]{1,0:T(8,128)(2,1)S(1)}, bf16[2048,256]{1,0:T(8,128)(2,1)}, u32[]{:S(2)}) copy-start(bf16[2048,256]{1,0:T(8,128)(2,1)} %param.7) | copy-start | bytes 3145732
  11.3 12.5 %copy-start.5 = (bf16[2048,256]{1,0:T(8,128)(2,1)S(1)}, bf16[2048,256]{1,0:T(8,128)(2,1)}, u32[]{:S(2)}) copy-start(bf16[2048,256]{1,0:T(8,128)(2,1)} %param.8) | copy-start | bytes 3145732
  33.8 43.3 %all-to-all-start.2 = ((bf16[4,512,384]{2,1,0:T(8,128)(2,1)}), bf16[4,512,384]{2,1,0:T(8,128)(2,1)S(1)}, u32[]{:S(2)}, u32[]{:S(2)}) async-start(bf16[4,512,384]{2,1,0:T(8,128)(2,1)} %bitcast.11), calls=%async_computation.2 | async-start | bytes 3145728 | tf_op jit(solution)/shard_map/all_to_all | solution.py:201
  77.1 3.6 %copy-start = (bf16[4,512,384]{2,1,0:T(8,128)(2,1)}, bf16[4,512,384]{2,1,0:T(8,128)(2,1)S(1)}, u32[]{:S(2)}) copy-start(bf16[4,512,384]{2,1,0:T(8,128)(2,1)S(1)} %all-to-all-done.2) | copy-start | bytes 4718596
  77.1 40.1 %all-to-all-start = ((bf16[4,512,384]{2,1,0:T(8,128)(2,1)}), bf16[4,512,384]{2,1,0:T(8,128)(2,1)S(1)}, u32[]{:S(2)}, u32[]{:S(2)}) async-start(bf16[4,512,384]{2,1,0:T(8,128)(2,1)} %bitcast.4), calls=%async_computation | async-start | bytes 3145728 | tf_op jit(solution)/shard_map/all_to_all | solution.py:201
  117.1 3.8 %copy-start.1 = (bf16[4,512,384]{2,1,0:T(8,128)(2,1)}, bf16[4,512,384]{2,1,0:T(8,128)(2,1)S(1)}, u32[]{:S(2)}) copy-start(bf16[4,512,384]{2,1,0:T(8,128)(2,1)S(1)} %all-to-all-done) | copy-start | bytes 4718596
  117.1 24.7 %all-to-all-start.3 = ((bf16[16,128,128]{2,1,0:T(8,128)(2,1)}), bf16[16,128,128]{2,1,0:T(8,128)(2,1)S(1)}, u32[]{:S(2)}, u32[]{:S(2)}) async-start(bf16[16,128,128]{2,1,0:T(8,128)(2,1)} %bitcast.15), calls=%async_computation.3 | async-start | bytes 1048576 | tf_op jit(solution)/shard_map/all_to_all | solution.py:210
  121.0 26.8 %copy-start.3 = (bf16[256,2048]{1,0:T(8,128)(2,1)S(1)}, bf16[256,2048]{1,0:T(8,128)(2,1)}, u32[]{:S(2)}) copy-start(bf16[256,2048]{1,0:T(8,128)(2,1)} %param.11) | copy-start | bytes 3145732
  121.0 26.8 %copy-start.6 = (f32[256]{0:T(256)S(1)}, f32[256]{0:T(256)}, u32[]{:S(2)}) copy-start(f32[256]{0:T(256)} %param.10) | copy-start | bytes 3076
  141.8 20.2 %all-to-all-start.1 = ((bf16[16,128,128]{2,1,0:T(8,128)(2,1)}), bf16[16,128,128]{2,1,0:T(8,128)(2,1)S(1)}, u32[]{:S(2)}, u32[]{:S(2)}) async-start(bf16[16,128,128]{2,1,0:T(8,128)(2,1)} %bitcast.8), calls=%async_computation.1 | async-start | bytes 1048576 | tf_op jit(solution)/shard_map/all_to_all | solution.py:210
  149.0 29.0 %collective-permute-start.2 = (bf16[256,2048]{1,0:T(8,128)(2,1)}, bf16[256,2048]{1,0:T(8,128)(2,1)}, u32[]{:S(2)}, u32[]{:S(2)}) collective-permute-start(bf16[256,2048]{1,0:T(8,128)(2,1)} %multiply_convert_fusion.1), channel_id=1, source_target_pairs={{0,3},{1,0},{2,1},{3,2},{4,7},{5,4},{6,5},{7,6},{8,11},{9,8},{10,9... | collective-permute-start | bytes 3145736 | tf_op jit(solution)/shard_map/ppermute | solution.py:182
  150.6 50.9 %collective-permute-start.1 = (bf16[256,2048]{1,0:T(8,128)(2,1)}, bf16[256,2048]{1,0:T(8,128)(2,1)}, u32[]{:S(2)}, u32[]{:S(2)}) collective-permute-start(bf16[256,2048]{1,0:T(8,128)(2,1)} %multiply_convert_fusion.1), channel_id=1, source_target_pairs={{0,2},{1,3},{2,0},{3,1},{4,6},{5,7},{6,4},{7,5},{8,10},{9,11},{10,... | collective-permute-start | bytes 3145736 | tf_op jit(solution)/shard_map/ppermute | solution.py:182
  151.0 50.5 %collective-permute-start = (bf16[256,2048]{1,0:T(8,128)(2,1)}, bf16[256,2048]{1,0:T(8,128)(2,1)}, u32[]{:S(2)}, u32[]{:S(2)}) collective-permute-start(bf16[256,2048]{1,0:T(8,128)(2,1)} %multiply_convert_fusion.1), channel_id=1, source_target_pairs={{0,1},{1,2},{2,3},{3,0},{4,5},{5,6},{6,7},{7,4},{8,9},{9,10},{10,1... | collective-permute-start | bytes 3145736 | tf_op jit(solution)/shard_map/ppermute | solution.py:182
where the time goes:
time: 209 us; the launch traced here: 208 us
  waiting for transfers between devices  87.6 us (42%)
  local copies, waits for them, and re-layouts  37.8 us (18%)
  Pallas kernels  37.6 us (18%)
  starting transfers between devices  21.8 us (10%)
  matrix products  19 us (9%)
  other arithmetic  4.25 us (2%)
    all_to_all x2, waiting for transfers between devices, body(): lax.all_to_all(product, 'sp', split_axis=0, concat_axis=0, tiled=True)  43.7 us
    pallas_call x2, Pallas kernels, attend_all(): pl.pallas_call(attend_kernel, grid=(batches, pairs), in_specs=[pl.BlockSp...  37.6 us
    ppermute x3, waiting for transfers between devices, body(): gathered.append(lax.ppermute(own, 'tp', route))  34 us
    dot_general x2, matrix products, body(): jnp.dot(flat, jnp.concatenate(columns, axis=1), preferred_element_type=jn...  14.5 us
    transpose x1, local copies, waits for them, and re-layouts, body(): tokens.reshape(per_class, CLASSES, batch_size, features)  11.5 us
    unnamed x15, local copies, waits for them, and re-layouts  11.3 us
    all_to_all x2, starting transfers between devices, body(): lax.all_to_all(product, 'sp', split_axis=0, concat_axis=0, tiled=True)  9.91 us
    all_to_all x2, waiting for transfers between devices, body(): lax.all_to_all(back, ('sp', 'tp'), split_axis=0, concat_axis=0, tiled=True)  9.81 us
  transfers between devices with their start and end apart: 7, of which 5 were waited for; matrix products, arithmetic and copies ran while one was open for 10% of the time, Pallas kernels for 18%

commit v1 on v0

--- a/solution.py
+++ b/solution.py
@@ -11,6 +11,7 @@
 PATTERNS = ((128, 1), (512, 4), (2048, 16))
 REACH = 128
 CLASSES = 16
+LANES = 128
 EPSILON = 1e-06
 NEGATIVE = -1e30
 GROUPS = 2
@@ -163,6 +164,56 @@
     )(*operands)
 
 
+def project_kernel(tokens_ref, weight_ref, *refs):
+    *out_refs, product = refs
+    step = pl.program_id(0)
+    positions, batch_size, features = tokens_ref.shape
+    rows = positions * batch_size
+    flat = tokens_ref[...].reshape(rows, features)
+    at = pl.ds(pl.multiple_of(step * rows, rows), rows)
+    total = jnp.dot(flat, weight_ref[...], preferred_element_type=jnp.float32)
+    for part in range(product.shape[0]):
+        product[part, at, :] = total[:, part * LANES : (part + 1) * LANES]
+
+    @pl.when(step == pl.num_programs(0) - 1)
+    def leave():
+        parts = product.shape[0] // len(out_refs)
+        per_class = out_refs[0].shape[2]
+
+        @pl.loop(0, CLASSES)
+        def of_class(c):
+            for part in range(product.shape[0]):
+                out_ref, first = out_refs[part // parts], part % parts * LANES
+                for b in range(batch_size):
+                    picked = pl.ds(c * batch_size + b, per_class, stride=CLASSES * batch_size)
+                    out_ref[b, c, :, first : first + LANES] = product[part, picked, :].astype(out_ref.dtype)
+
+
+def project(tokens, weight, groups):
+    seq_rows, batch_size, features = tokens.shape
+    columns = weight.shape[1]
+    per_class = seq_rows // CLASSES
+    block = min(64, seq_rows)
+    shape = (batch_size, CLASSES, per_class, columns // groups)
+    return pl.pallas_call(
+        project_kernel,
+        grid=(seq_rows // block,),
+        in_specs=[
+            pl.BlockSpec((block, batch_size, features), lambda i: (i, 0, 0)),
+            pl.BlockSpec(weight.shape, lambda i: (0, 0)),
+        ],
+        out_specs=[pl.BlockSpec(shape, lambda i: (0, 0, 0, 0))] * groups,
+        out_shape=[jax.ShapeDtypeStruct(shape, jnp.bfloat16)] * groups,
+        scratch_shapes=[pltpu.VMEM((columns // LANES, seq_rows * batch_size, LANES), jnp.float32)],
+        compiler_params=pltpu.CompilerParams(dimension_semantics=("arbitrary",)),
+        cost_estimate=pl.CostEstimate(
+            flops=2 * seq_rows * batch_size * features * columns,
+            bytes_accessed=2 * (tokens.size + weight.size + seq_rows * batch_size * columns),
+            transcendentals=0,
+        ),
+    )(tokens, weight)
+
+
 def body(tokens, query_weight, key_weight, value_weight, mix_gain, out_weight):
     seq_rows, batch_size, features = tokens.shape
     channels = query_weight.shape[1]
@@ -176,29 +227,29 @@
     groups = GROUPS if head_split == 1 else 1
 
     own = (out_weight.astype(jnp.float32) * mix_gain[:, None]).astype(jnp.bfloat16)
-    gathered = [own]
-    for step in range(1, tp_count):
-        route = [(i, (i + step) % tp_count) for i in range(tp_count)]
-        gathered.append(lax.ppermute(own, "tp", route))
-
-    flat = tokens.reshape(per_class, CLASSES, batch_size, features).transpose(2, 1, 0, 3)
-    flat = flat.reshape(batch_size * seq_rows, features)
+    gathered, sources, step = own, [0], tp_count // 2
+    while step:
+        route = [(i, i ^ step) for i in range(tp_count)]
+        gathered = jnp.concatenate([gathered, lax.ppermute(gathered, "tp", route)], axis=0)
+        sources += [s ^ step for s in sources]
+        step //= 2
+
     cut = channels // groups // head_split
     width = min(cut, 2 * HEAD_DIM)
+    columns = []
+    for g in range(groups * head_split):
+        columns += [w[:, g * cut : (g + 1) * cut] for w in (query_weight, key_weight, value_weight)]
+    products = project(tokens, jnp.concatenate(columns, axis=1), groups)
     results = []
-    for g in range(groups):
-        columns = []
-        for s in range(head_split):
-            at = (g * head_split + s) * cut
-            columns += [w[:, at : at + cut] for w in (query_weight, key_weight, value_weight)]
-        product = jnp.dot(flat, jnp.concatenate(columns, axis=1), preferred_element_type=jnp.float32)
-        product = product.astype(jnp.bfloat16).reshape(batch_size, seq_rows, head_split, 3 * cut)
+    for g, product in enumerate(products):
         if head_split > 1:
-            product = product.transpose(0, 2, 1, 3)
+            product = product.reshape(batch_size, seq_rows, head_split, 3 * cut).transpose(0, 2, 1, 3)
         product = product.reshape(sp_count // copies, batches * seq_rows, 3 * cut)
         if copies > 1:
             product = jnp.repeat(product, copies, axis=0)
         moved = lax.all_to_all(product, "sp", split_axis=0, concat_axis=0, tiled=True)
+        if g == 0:
+            moved, gathered = lax.optimization_barrier((moved, gathered))
         moved = moved.reshape(sp_count, batches, CLASSES, per_class, 3 * cut)
         results.append(attend_all(moved, width))
 
@@ -213,14 +264,12 @@
     combined = jnp.stack(backs, axis=0).transpose(3, 6, 5, 1, 4, 0, 2, 7)
     rows = part * CLASSES * batch_size
     combined = combined.reshape(tp_count, rows, channels)
-    flipped = combined[::-1]
-    turned = lax.dynamic_slice_in_dim(
-        jnp.concatenate([flipped, flipped], axis=0), tp_count - 1 - tp_place, tp_count, axis=0
+    turned = jnp.concatenate(
+        [lax.dynamic_index_in_dim(combined, tp_place ^ s, axis=0, keepdims=False) for s in sources], axis=1
     )
-    turned = turned.transpose(1, 0, 2).reshape(rows, tp_count * channels)
     wide = turned.astype(jnp.float32)
     row_scale = lax.rsqrt(jnp.mean(wide * wide, axis=-1, keepdims=True) + EPSILON)
-    mixed = jnp.dot(turned, jnp.concatenate(gathered, axis=0), preferred_element_type=jnp.float32) * row_scale
+    mixed = jnp.dot(turned, gathered, preferred_element_type=jnp.float32) * row_scale
     return mixed.astype(jnp.bfloat16).reshape(part * CLASSES, batch_size, out_weight.shape[1])
 
 

time: 209 us -> 167 us (0.80)
  waiting for transfers between devices: 87.6 us -> 62.8 us
  local copies, waits for them, and re-layouts: 37.8 us -> 14.7 us
  Pallas kernels: 37.6 us -> 53.9 us
  matrix products: 19 us -> 4.55 us
  other arithmetic: 4.25 us -> 7.87 us
    ppermute x3 -> x2, waiting for transfers between devices: 34 us -> 0.01 us  [body(): lax.ppermute(gathered, 'tp', route)]
    pallas_call x0 -> x1, Pallas kernels: none -> 16.4 us  [project(): pl.pallas_call(project_kernel, grid=(seq_rows // block,), in_specs=[pl.Bl...]
    dot_general x3 -> x1, matrix products: 19 us -> 4.55 us  [body(): jnp.dot(turned, gathered, preferred_element_type=jnp.float32) * row_scale]
    transpose x2 -> x0, local copies, waits for them, and re-layouts: 12.1 us -> none  [the longest x1 11.5 us: body(): tokens.reshape(per_class, CLASSES, batch_size, features)]
    all_to_all x2, waiting for transfers between devices: 43.7 us -> 49.6 us  [body(): lax.all_to_all(product, 'sp', split_axis=0, concat_axis=0, tiled=True)]
    unnamed x15 -> x17, local copies, waits for them, and re-layouts: 11.3 us -> 5.52 us
    concatenate x0 -> x2, other arithmetic: none -> 4.91 us  [body(): jnp.concatenate([gathered, lax.ppermute(gathered, 'tp', route)], axis=0)]
    all_to_all x2, waiting for transfers between devices: 9.81 us -> 13.2 us  [body(): lax.all_to_all(back, ('sp', 'tp'), split_axis=0, concat_axis=0, tiled=True)]
  transfers between devices with their start and end apart: 7 -> 6, of which waited for: 5 -> 3; matrix products, arithmetic and copies ran while one was open for 10% -> 6% of each run, Pallas kernels for 18% -> 23%
where the time goes in v1:
time: 167 us; the launch traced here: 166 us
  waiting for transfers between devices  62.8 us (38%)
  Pallas kernels  53.9 us (32%)
  starting transfers between devices  22.2 us (13%)
  local copies, waits for them, and re-layouts  14.7 us (9%)
  other arithmetic  7.87 us (5%)
  matrix products  4.55 us (3%)
    all_to_all x2, waiting for transfers between devices, body(): lax.all_to_all(product, 'sp', split_axis=0, concat_axis=0, tiled=True)  49.6 us
    pallas_call x2, Pallas kernels, attend_all(): pl.pallas_call(attend_kernel, grid=(batches, pairs), in_specs=[pl.BlockSp...  37.5 us
    pallas_call x1, Pallas kernels, project(): pl.pallas_call(project_kernel, grid=(seq_rows // block,), in_specs=[pl.Bl...  16.4 us
    all_to_all x2, waiting for transfers between devices, body(): lax.all_to_all(back, ('sp', 'tp'), split_axis=0, concat_axis=0, tiled=True)  13.2 us
    all_to_all x2, starting transfers between devices, body(): lax.all_to_all(product, 'sp', split_axis=0, concat_axis=0, tiled=True)  10.8 us
    all_to_all x2, starting transfers between devices, body(): lax.all_to_all(back, ('sp', 'tp'), split_axis=0, concat_axis=0, tiled=True)  9.77 us
    unnamed x17, local copies, waits for them, and re-layouts  5.52 us
    concatenate x2, other arithmetic, body(): jnp.concatenate([gathered, lax.ppermute(gathered, 'tp', route)], axis=0)  4.91 us
  transfers between devices with their start and end apart: 6, of which 3 were waited for; matrix products, arithmetic and copies ran while one was open for 6% of the time, Pallas kernels for 23%

profile of v1, /device:TPU:0, one launch (start us, length us, event | category | flops | bytes accessed | tf_op | source)
XLA Modules:
  0.0 166.2 jit_solution(18315856705372709418)
XLA Ops:
  0.0 1.3 slice_dynamic-update-slice_fusion.5
  1.3 1.2 slice_dynamic-update-slice_fusion.4
  2.5 1.2 slice_dynamic-update-slice_fusion.3
  3.6 0.1 slice_dynamic-update-slice_fusion.2
  3.8 0.1 slice_dynamic-update-slice_fusion.1
  3.9 0.1 slice_dynamic-update-slice_fusion.weight_ref
  4.1 1.6 copy-done.4
  5.7 16.4 %shard_map.64 = (bf16[4,16,32,384]{3,2,1,0:T(8,128)(2,1)}, bf16[4,16,32,384]{3,2,1,0:T(8,128)(2,1)}) custom-call(bf16[512,4,2048]{2,1,0:T(4,128)(2,1)} %tokens_ref.1, bf16[2048,768]{1,0:T(8,128)(2,1)} %copy-done.4), custom_call_target="tpu_custom_call" | custom-call | flops 6442450944 | bytes 14680064 | tf_op jit(solution)/shard_map/pallas_call | solution.py:198
  22.1 6.5 %all-to-all-start.2 = ((bf16[4,512,384]{2,1,0:T(8,128)(2,1)}), bf16[4,512,384]{2,1,0:T(8,128)(2,1)}, u32[]{:S(2)}, u32[]{:S(2)}) async-start(bf16[4,512,384]{2,1,0:T(8,128)(2,1)} %bitcast.30), calls=%async_computation.2 | async-start | bytes 3145728 | tf_op jit(solution)/shard_map/all_to_all | solution.py:250
  28.6 0.2 multiply_convert_fusion.1
  28.9 1.6 collective-permute-start
  30.4 35.3 %all-to-all-done.2 = bf16[4,512,384]{2,1,0:T(8,128)(2,1)} async-done(((bf16[4,512,384]{2,1,0:T(8,128)(2,1)}), bf16[4,512,384]{2,1,0:T(8,128)(2,1)}, u32[]{:S(2)}, u32[]{:S(2)}) %all-to-all-start.2) | async-done | bytes 1572896 | tf_op jit(solution)/shard_map/all_to_all | solution.py:250
  65.7 4.4 %all-to-all-start = ((bf16[4,512,384]{2,1,0:T(8,128)(2,1)}), bf16[4,512,384]{2,1,0:T(8,128)(2,1)}, u32[]{:S(2)}, u32[]{:S(2)}) async-start(bf16[4,512,384]{2,1,0:T(8,128)(2,1)} %bitcast.29), calls=%async_computation | async-start | bytes 3145728 | tf_op jit(solution)/shard_map/all_to_all | solution.py:250
  70.1 0.0 collective-permute-done
  70.1 1.5 pad_maximum_fusion.1
  71.5 18.8 %shard_map.66 = bf16[4,1,16,32,128]{4,3,2,1,0:T(8,128)(2,1)} custom-call(bf16[4,1,16,32,384]{4,3,2,1,0:T(8,128)(2,1)} %bitcast.7.q_ref.k_ref.v_ref, bf16[4,1,16,32,384]{4,3,2,1,0:T(8,128)(2,1)} %bitcast.7.q_ref.k_ref.v_ref, bf16[4,1,16,32,384]{4,3,2,1,0:T(8,128)(2,1)} %bitcast.7.q_ref.k_ref.v_ref), custom_call_target="tpu_custom_call" | custom-call | flops 943718400 | bytes 2097152 | tf_op jit(solution)/shard_map/pallas_call | solution.py:145
  90.3 2.0 %copy.8 = bf16[4,1,16,4,8,128]{5,4,2,3,0,1:T(8,128)(2,1)} copy(bf16[4,1,16,4,8,128]{5,4,3,2,0,1:T(8,128)(2,1)} %bitcast.31) | data formatting | bytes 1048576 | tf_op jit(solution)/shard_map/reshape | solution.py:259
  92.3 14.4 %all-to-all-done = bf16[4,512,384]{2,1,0:T(8,128)(2,1)} async-done(((bf16[4,512,384]{2,1,0:T(8,128)(2,1)}), bf16[4,512,384]{2,1,0:T(8,128)(2,1)}, u32[]{:S(2)}, u32[]{:S(2)}) %all-to-all-start) | async-done | bytes 1572896 | tf_op jit(solution)/shard_map/all_to_all | solution.py:250
  106.6 3.8 %all-to-all-start.3 = ((bf16[16,128,128]{2,1,0:T(8,128)(2,1)}), bf16[16,128,128]{2,1,0:T(8,128)(2,1)S(1)}, u32[]{:S(2)}, u32[]{:S(2)}) async-start(bf16[16,128,128]{2,1,0:T(8,128)(2,1)} %bitcast.10), calls=%async_computation.3 | async-start | bytes 1048576 | tf_op jit(solution)/shard_map/all_to_all | solution.py:261
  110.4 3.5 %pad_maximum_fusion = bf16[1024,2048]{1,0:T(8,128)(2,1)} fusion(bf16[512,2048]{1,0:T(8,128)(2,1)} %collective-permute-done.1, bf16[256,2048]{1,0:T(8,128)(2,1)S(1)} %collective-permute-done, bf16[256,2048]{1,0:T(8,128)(2,1)S(1)} %multiply_convert_fusion.1), kind=kLoop, calls=%fused_computation | loop fusion | flops 12582912 | bytes 8388608 | tf_op jit(solution)/shard_map/concatenate | solution.py:233
  113.9 18.8 %shard_map.65 = bf16[4,1,16,32,128]{4,3,2,1,0:T(8,128)(2,1)} custom-call(bf16[4,1,16,32,384]{4,3,2,1,0:T(8,128)(2,1)} %bitcast.1.q_ref.k_ref.v_ref, bf16[4,1,16,32,384]{4,3,2,1,0:T(8,128)(2,1)} %bitcast.1.q_ref.k_ref.v_ref, bf16[4,1,16,32,384]{4,3,2,1,0:T(8,128)(2,1)} %bitcast.1.q_ref.k_ref.v_ref), custom_call_target="tpu_custom_call" | custom-call | flops 943718400 | bytes 2097152 | tf_op jit(solution)/shard_map/pallas_call | solution.py:145
  132.6 2.0 %copy.7 = bf16[4,1,16,4,8,128]{5,4,2,3,0,1:T(8,128)(2,1)} copy(bf16[4,1,16,4,8,128]{5,4,3,2,0,1:T(8,128)(2,1)} %bitcast.32) | data formatting | bytes 1048576 | tf_op jit(solution)/shard_map/reshape | solution.py:259
  134.6 6.0 %all-to-all-start.1 = ((bf16[16,128,128]{2,1,0:T(8,128)(2,1)}), bf16[16,128,128]{2,1,0:T(8,128)(2,1)S(1)}, u32[]{:S(2)}, u32[]{:S(2)}) async-start(bf16[16,128,128]{2,1,0:T(8,128)(2,1)} %bitcast.4), calls=%async_computation.1 | async-start | bytes 1048576 | tf_op jit(solution)/shard_map/all_to_all | solution.py:261
  140.6 1.1 copy.10
  141.7 13.2 %all-to-all-done.1 = bf16[16,128,128]{2,1,0:T(8,128)(2,1)S(1)} async-done(((bf16[16,128,128]{2,1,0:T(8,128)(2,1)}), bf16[16,128,128]{2,1,0:T(8,128)(2,1)S(1)}, u32[]{:S(2)}, u32[]{:S(2)}) %all-to-all-start.1) | async-done | bytes 524320 | tf_op jit(solution)/shard_map/all_to_all | solution.py:261
  154.9 1.1 copy.9
  156.0 2.4 %maximum_bitcast_fusion = bf16[4,8,16,4,1,2,1,128]{7,5,3,2,1,0,6,4:T(2,128)(2,1)S(1)} fusion(bf16[1,4,1,4,1,16,8,128]{7,0,1,5,6,3,2,4:T(2,128)(2,1)S(1)} %copy.10, bf16[1,4,1,4,1,16,8,128]{7,0,1,5,6,3,2,4:T(2,128)(2,1)S(1)} %copy.9), kind=kLoop, calls=%fused_computation.5 | loop fusion | flops 2097152 | bytes 2097152 | tf_op jit(solution)/shard_map/transpose | solution.py:264
  158.4 0.7 reshape.47
  159.1 0.1 dynamic-slice_bitcast_fusion.3
  159.2 0.3 multiply_reduce_fusion
  159.5 4.5 %multiply_convert_fusion = bf16[512,2048]{1,0:T(8,128)(2,1)S(1)} fusion(bf16[1024,2048]{1,0:T(8,128)(2,1)} %pad_maximum_fusion, f32[512]{0:T(512)S(1)} %add_rsqrt_fusion, bf16[512,256]{1,0:T(8,128)(2,1)S(1)} %get-tuple-element.14, bf16[512,256]{1,0:T(8,128)(2,1)S(1)} %get-tuple-element.15, bf16[512,256]{1,0:T(8,128)(2,1)S(1)} %get-tuple-element.16, ...), kind=kOutput, calls=%fused_computation.1 | convolution fusion | flops 2153775104 | bytes 7342080 | tf_op jit(solution)/shard_map/dot_general | solution.py:272
  164.0 2.2 %reshape.48 = bf16[128,4,2048]{2,1,0:T(4,128)(2,1)} reshape(bf16[512,2048]{1,0:T(8,128)(2,1)S(1)} %multiply_convert_fusion) | data formatting | bytes 4194304 | tf_op jit(solution)/shard_map/reshape | solution.py:273
  (15 shorter events, 0.0 us)
Async XLA Ops:
  0.0 3.6 %copy-start = (bf16[2048,256]{1,0:T(8,128)(2,1)S(1)}, bf16[2048,256]{1,0:T(8,128)(2,1)}, u32[]{:S(2)}) copy-start(bf16[2048,256]{1,0:T(8,128)(2,1)} %param.7) | copy-start | bytes 3145732
  0.0 3.8 %copy-start.1 = (bf16[2048,256]{1,0:T(8,128)(2,1)S(1)}, bf16[2048,256]{1,0:T(8,128)(2,1)}, u32[]{:S(2)}) copy-start(bf16[2048,256]{1,0:T(8,128)(2,1)} %param.8) | copy-start | bytes 3145732
  0.0 3.9 %copy-start.2 = (bf16[2048,256]{1,0:T(8,128)(2,1)S(1)}, bf16[2048,256]{1,0:T(8,128)(2,1)}, u32[]{:S(2)}) copy-start(bf16[2048,256]{1,0:T(8,128)(2,1)} %param.9) | copy-start | bytes 3145732
  4.1 1.6 copy-start.4
  22.1 6.5 %copy-start.3 = (bf16[256,2048]{1,0:T(8,128)(2,1)S(1)}, bf16[256,2048]{1,0:T(8,128)(2,1)}, u32[]{:S(2)}) copy-start(bf16[256,2048]{1,0:T(8,128)(2,1)} %param.11) | copy-start | bytes 3145732
  22.1 6.5 %copy-start.5 = (f32[256]{0:T(256)S(1)}, f32[256]{0:T(256)}, u32[]{:S(2)}) copy-start(f32[256]{0:T(256)} %param.10) | copy-start | bytes 3076
  22.1 43.5 %all-to-all-start.2 = ((bf16[4,512,384]{2,1,0:T(8,128)(2,1)}), bf16[4,512,384]{2,1,0:T(8,128)(2,1)}, u32[]{:S(2)}, u32[]{:S(2)}) async-start(bf16[4,512,384]{2,1,0:T(8,128)(2,1)} %bitcast.30), calls=%async_computation.2 | async-start | bytes 3145728 | tf_op jit(solution)/shard_map/all_to_all | solution.py:250
  28.9 41.2 %collective-permute-start = (bf16[256,2048]{1,0:T(8,128)(2,1)S(1)}, bf16[256,2048]{1,0:T(8,128)(2,1)S(1)}, u32[]{:S(2)}, u32[]{:S(2)}) collective-permute-start(bf16[256,2048]{1,0:T(8,128)(2,1)S(1)} %multiply_convert_fusion.1), channel_id=1, source_target_pairs={{0,2},{1,3},{2,0},{3,1},{4,6},{5,7},{6,4},{7,5},{8,10},{9,11},{10,... | collective-permute-start | bytes 3145736 | tf_op jit(solution)/shard_map/ppermute | solution.py:233
  65.7 41.0 %all-to-all-start = ((bf16[4,512,384]{2,1,0:T(8,128)(2,1)}), bf16[4,512,384]{2,1,0:T(8,128)(2,1)}, u32[]{:S(2)}, u32[]{:S(2)}) async-start(bf16[4,512,384]{2,1,0:T(8,128)(2,1)} %bitcast.29), calls=%async_computation | async-start | bytes 3145728 | tf_op jit(solution)/shard_map/all_to_all | solution.py:250
  71.5 38.9 %collective-permute-start.1 = (bf16[512,2048]{1,0:T(8,128)(2,1)}, bf16[512,2048]{1,0:T(8,128)(2,1)}, u32[]{:S(2)}, u32[]{:S(2)}) collective-permute-start(bf16[512,2048]{1,0:T(8,128)(2,1)} %pad_maximum_fusion.1), channel_id=1, source_target_pairs={{0,1},{1,0},{2,3},{3,2},{4,5},{5,4},{6,7},{7,6},{8,9},{9,8},{10,11... | collective-permute-start | bytes 6291464 | tf_op jit(solution)/shard_map/ppermute | solution.py:233
  106.6 28.0 %all-to-all-start.3 = ((bf16[16,128,128]{2,1,0:T(8,128)(2,1)}), bf16[16,128,128]{2,1,0:T(8,128)(2,1)S(1)}, u32[]{:S(2)}, u32[]{:S(2)}) async-start(bf16[16,128,128]{2,1,0:T(8,128)(2,1)} %bitcast.10), calls=%async_computation.3 | async-start | bytes 1048576 | tf_op jit(solution)/shard_map/all_to_all | solution.py:261
  134.6 20.3 %all-to-all-start.1 = ((bf16[16,128,128]{2,1,0:T(8,128)(2,1)}), bf16[16,128,128]{2,1,0:T(8,128)(2,1)S(1)}, u32[]{:S(2)}, u32[]{:S(2)}) async-start(bf16[16,128,128]{2,1,0:T(8,128)(2,1)} %bitcast.4), calls=%async_computation.1 | async-start | bytes 1048576 | tf_op jit(solution)/shard_map/all_to_all | solution.py:261

commit v2 on v1

--- a/solution.py
+++ b/solution.py
@@ -164,54 +164,53 @@
     )(*operands)
 
 
-def project_kernel(tokens_ref, weight_ref, *refs):
-    *out_refs, product = refs
+def project_kernel(weight_count, places, tokens_ref, *refs):
+    weight_refs, out_ref, product = refs[:weight_count], refs[weight_count], refs[-1]
     step = pl.program_id(0)
     positions, batch_size, features = tokens_ref.shape
     rows = positions * batch_size
     flat = tokens_ref[...].reshape(rows, features)
     at = pl.ds(pl.multiple_of(step * rows, rows), rows)
-    total = jnp.dot(flat, weight_ref[...], preferred_element_type=jnp.float32)
-    for part in range(product.shape[0]):
-        product[part, at, :] = total[:, part * LANES : (part + 1) * LANES]
+    for weight_ref, parts in zip(weight_refs, places):
+        total = jnp.dot(flat, weight_ref[...], preferred_element_type=jnp.float32)
+        for i, part in enumerate(parts):
+            product[part, at, :] = total[:, i * LANES : (i + 1) * LANES]
 
     @pl.when(step == pl.num_programs(0) - 1)
     def leave():
-        parts = product.shape[0] // len(out_refs)
-        per_class = out_refs[0].shape[2]
+        per_class = out_ref.shape[2]
 
         @pl.loop(0, CLASSES)
         def of_class(c):
             for part in range(product.shape[0]):
-                out_ref, first = out_refs[part // parts], part % parts * LANES
                 for b in range(batch_size):
                     picked = pl.ds(c * batch_size + b, per_class, stride=CLASSES * batch_size)
-                    out_ref[b, c, :, first : first + LANES] = product[part, picked, :].astype(out_ref.dtype)
-
-
-def project(tokens, weight, groups):
+                    out_ref[b, c, :, part * LANES : (part + 1) * LANES] = product[part, picked, :].astype(out_ref.dtype)
+
+
+def project(tokens, weights, group, cut):
     seq_rows, batch_size, features = tokens.shape
-    columns = weight.shape[1]
+    columns = cut * len(weights)
     per_class = seq_rows // CLASSES
     block = min(64, seq_rows)
-    shape = (batch_size, CLASSES, per_class, columns // groups)
+    shape = (batch_size, CLASSES, per_class, columns)
+    each = cut // LANES
+    places = [range(w * each, (w + 1) * each) for w in range(len(weights))]
     return pl.pallas_call(
-        project_kernel,
+        functools.partial(project_kernel, len(weights), places),
         grid=(seq_rows // block,),
-        in_specs=[
-            pl.BlockSpec((block, batch_size, features), lambda i: (i, 0, 0)),
-            pl.BlockSpec(weight.shape, lambda i: (0, 0)),
-        ],
-        out_specs=[pl.BlockSpec(shape, lambda i: (0, 0, 0, 0))] * groups,
-        out_shape=[jax.ShapeDtypeStruct(shape, jnp.bfloat16)] * groups,
+        in_specs=[pl.BlockSpec((block, batch_size, features), lambda i: (i, 0, 0))]
+        + [pl.BlockSpec((features, cut), lambda i: (0, group))] * len(weights),
+        out_specs=pl.BlockSpec(shape, lambda i: (0, 0, 0, 0)),
+        out_shape=jax.ShapeDtypeStruct(shape, jnp.bfloat16),
         scratch_shapes=[pltpu.VMEM((columns // LANES, seq_rows * batch_size, LANES), jnp.float32)],
         compiler_params=pltpu.CompilerParams(dimension_semantics=("arbitrary",)),
         cost_estimate=pl.CostEstimate(
             flops=2 * seq_rows * batch_size * features * columns,
-            bytes_accessed=2 * (tokens.size + weight.size + seq_rows * batch_size * columns),
+            bytes_accessed=2 * (tokens.size + features * columns + seq_rows * batch_size * columns),
             transcendentals=0,
         ),
-    )(tokens, weight)
+    )(tokens, *weights)
 
 
 def body(tokens, query_weight, key_weight, value_weight, mix_gain, out_weight):
@@ -236,12 +235,15 @@
 
     cut = channels // groups // head_split
     width = min(cut, 2 * HEAD_DIM)
-    columns = []
-    for g in range(groups * head_split):
-        columns += [w[:, g * cut : (g + 1) * cut] for w in (query_weight, key_weight, value_weight)]
-    products = project(tokens, jnp.concatenate(columns, axis=1), groups)
+    weights = (query_weight, key_weight, value_weight)
     results = []
-    for g, product in enumerate(products):
+    for g in range(groups):
+        if cut % LANES == 0 and head_split == 1:
+            product = project(tokens, weights, g, cut)
+        else:
+            spans = [slice(i * cut, (i + 1) * cut) for i in range(g * head_split, (g + 1) * head_split)]
+            whole = jnp.concatenate([w[:, span] for span in spans for w in weights], axis=1)
+            product = project(tokens, (whole,), 0, whole.shape[1])
         if head_split > 1:
             product = product.reshape(batch_size, seq_rows, head_split, 3 * cut).transpose(0, 2, 1, 3)
         product = product.reshape(sp_count // copies, batches * seq_rows, 3 * cut)

time: 167 us -> 159 us (0.952)
  waiting for transfers between devices: 62.8 us -> 49.3 us
  Pallas kernels: 53.9 us -> 64.4 us
  local copies, waits for them, and re-layouts: 14.7 us -> 9.14 us
    all_to_all x2, waiting for transfers between devices: 49.6 us -> 36.1 us  [body(): lax.all_to_all(product, 'sp', split_axis=0, concat_axis=0, tiled=True)]
    pallas_call x1 -> x2, Pallas kernels: 16.4 us -> 27 us  [project(): pl.pallas_call(functools.partial(project_kernel, len(weights), places), g...]
    unnamed x17 -> x4, local copies, waits for them, and re-layouts: 5.52 us -> 0.01 us
  transfers between devices with their start and end apart: 6 -> 6, of which waited for: 3 -> 3; matrix products, arithmetic and copies ran while one was open for 6% -> 6% of each run, Pallas kernels for 23% -> 32%
where the time goes in v2:
time: 159 us; the launch traced here: 158 us
  Pallas kernels  64.4 us (41%)
  waiting for transfers between devices  49.3 us (31%)
  starting transfers between devices  22.2 us (14%)
  local copies, waits for them, and re-layouts  9.14 us (6%)
  other arithmetic  7.86 us (5%)
  matrix products  4.55 us (3%)
    pallas_call x2, Pallas kernels, attend_all(): pl.pallas_call(attend_kernel, grid=(batches, pairs), in_specs=[pl.BlockSp...  37.5 us
    all_to_all x2, waiting for transfers between devices, body(): lax.all_to_all(product, 'sp', split_axis=0, concat_axis=0, tiled=True)  36.1 us
    pallas_call x2, Pallas kernels, project(): pl.pallas_call(functools.partial(project_kernel, len(weights), places), g...  27 us
    all_to_all x2, waiting for transfers between devices, body(): lax.all_to_all(back, ('sp', 'tp'), split_axis=0, concat_axis=0, tiled=True)  13.2 us
    all_to_all x2, starting transfers between devices, body(): lax.all_to_all(product, 'sp', split_axis=0, concat_axis=0, tiled=True)  10.8 us
    all_to_all x2, starting transfers between devices, body(): lax.all_to_all(back, ('sp', 'tp'), split_axis=0, concat_axis=0, tiled=True)  9.81 us
    concatenate x2, other arithmetic, body(): jnp.concatenate([gathered, lax.ppermute(gathered, 'tp', route)], axis=0)  4.9 us
    dot_general x1, matrix products, body(): jnp.dot(turned, gathered, preferred_element_type=jnp.float32) * row_scale  4.55 us
  transfers between devices with their start and end apart: 6, of which 3 were waited for; matrix products, arithmetic and copies ran while one was open for 6% of the time, Pallas kernels for 32%

profile of v2, /device:TPU:0, one launch (start us, length us, event | category | flops | bytes accessed | tf_op | source)
XLA Modules:
  0.0 157.6 jit_solution(17482887396283003568)
XLA Ops:
  0.0 13.5 %shard_map.66 = bf16[4,16,32,384]{3,2,1,0:T(8,128)(2,1)} custom-call(bf16[512,4,2048]{2,1,0:T(4,128)(2,1)} %tokens_ref.3, bf16[2048,256]{1,0:T(8,128)(2,1)} %refs_0_.3, bf16[2048,256]{1,0:T(8,128)(2,1)} %refs_1_.3, bf16[2048,256]{1,0:T(8,128)(2,1)} %refs_2_.3), custom_call_target="tpu_custom_call" | custom-call | flops 3221225472 | bytes 11534336 | tf_op jit(solution)/shard_map/pallas_call | solution.py:199
  13.5 0.0 copy-start
  13.5 6.5 %all-to-all-start.2 = ((bf16[4,512,384]{2,1,0:T(8,128)(2,1)}), bf16[4,512,384]{2,1,0:T(8,128)(2,1)}, u32[]{:S(2)}, u32[]{:S(2)}) async-start(bf16[4,512,384]{2,1,0:T(8,128)(2,1)} %bitcast.28), calls=%async_computation.2 | async-start | bytes 3145728 | tf_op jit(solution)/shard_map/all_to_all | solution.py:252
  20.0 0.0 copy-done
  20.0 0.0 copy-done.1
  20.0 0.2 multiply_convert_fusion.1
  20.2 1.6 collective-permute-start
  21.8 13.5 %shard_map.64 = bf16[4,16,32,384]{3,2,1,0:T(8,128)(2,1)} custom-call(bf16[512,4,2048]{2,1,0:T(4,128)(2,1)} %tokens_ref.3, bf16[2048,256]{1,0:T(8,128)(2,1)} %refs_0_.3, bf16[2048,256]{1,0:T(8,128)(2,1)} %refs_1_.3, bf16[2048,256]{1,0:T(8,128)(2,1)} %refs_2_.3), custom_call_target="tpu_custom_call" | custom-call | flops 3221225472 | bytes 11534336 | tf_op jit(solution)/shard_map/pallas_call | solution.py:199
  35.2 21.8 %all-to-all-done.2 = bf16[4,512,384]{2,1,0:T(8,128)(2,1)} async-done(((bf16[4,512,384]{2,1,0:T(8,128)(2,1)}), bf16[4,512,384]{2,1,0:T(8,128)(2,1)}, u32[]{:S(2)}, u32[]{:S(2)}) %all-to-all-start.2) | async-done | bytes 1572896 | tf_op jit(solution)/shard_map/all_to_all | solution.py:252
  57.0 4.4 %all-to-all-start = ((bf16[4,512,384]{2,1,0:T(8,128)(2,1)}), bf16[4,512,384]{2,1,0:T(8,128)(2,1)}, u32[]{:S(2)}, u32[]{:S(2)}) async-start(bf16[4,512,384]{2,1,0:T(8,128)(2,1)} %bitcast.27), calls=%async_computation | async-start | bytes 3145728 | tf_op jit(solution)/shard_map/all_to_all | solution.py:252
  61.4 0.0 collective-permute-done
  61.4 1.5 pad_maximum_fusion.1
  62.9 0.0 collective-permute-start.1
  62.9 18.7 %shard_map.67 = bf16[4,1,16,32,128]{4,3,2,1,0:T(8,128)(2,1)} custom-call(bf16[4,1,16,32,384]{4,3,2,1,0:T(8,128)(2,1)} %bitcast.7.q_ref.k_ref.v_ref, bf16[4,1,16,32,384]{4,3,2,1,0:T(8,128)(2,1)} %bitcast.7.q_ref.k_ref.v_ref, bf16[4,1,16,32,384]{4,3,2,1,0:T(8,128)(2,1)} %bitcast.7.q_ref.k_ref.v_ref), custom_call_target="tpu_custom_call" | custom-call | flops 943718400 | bytes 2097152 | tf_op jit(solution)/shard_map/pallas_call | solution.py:145
  81.6 2.0 %copy.8 = bf16[4,1,16,4,8,128]{5,4,2,3,0,1:T(8,128)(2,1)} copy(bf16[4,1,16,4,8,128]{5,4,3,2,0,1:T(8,128)(2,1)} %bitcast.31) | data formatting | bytes 1048576 | tf_op jit(solution)/shard_map/reshape | solution.py:261
  83.6 14.3 %all-to-all-done = bf16[4,512,384]{2,1,0:T(8,128)(2,1)} async-done(((bf16[4,512,384]{2,1,0:T(8,128)(2,1)}), bf16[4,512,384]{2,1,0:T(8,128)(2,1)}, u32[]{:S(2)}, u32[]{:S(2)}) %all-to-all-start) | async-done | bytes 1572896 | tf_op jit(solution)/shard_map/all_to_all | solution.py:252
  98.0 3.8 %all-to-all-start.3 = ((bf16[16,128,128]{2,1,0:T(8,128)(2,1)}), bf16[16,128,128]{2,1,0:T(8,128)(2,1)S(1)}, u32[]{:S(2)}, u32[]{:S(2)}) async-start(bf16[16,128,128]{2,1,0:T(8,128)(2,1)} %bitcast.10), calls=%async_computation.3 | async-start | bytes 1048576 | tf_op jit(solution)/shard_map/all_to_all | solution.py:263
  101.8 0.0 collective-permute-done.1
  101.8 3.4 %pad_maximum_fusion = bf16[1024,2048]{1,0:T(8,128)(2,1)} fusion(bf16[512,2048]{1,0:T(8,128)(2,1)} %collective-permute-done.1, bf16[256,2048]{1,0:T(8,128)(2,1)S(1)} %collective-permute-done, bf16[256,2048]{1,0:T(8,128)(2,1)S(1)} %multiply_convert_fusion.1), kind=kLoop, calls=%fused_computation | loop fusion | flops 12582912 | bytes 8388608 | tf_op jit(solution)/shard_map/concatenate | solution.py:232
  105.2 18.7 %shard_map.65 = bf16[4,1,16,32,128]{4,3,2,1,0:T(8,128)(2,1)} custom-call(bf16[4,1,16,32,384]{4,3,2,1,0:T(8,128)(2,1)} %bitcast.1.q_ref.k_ref.v_ref, bf16[4,1,16,32,384]{4,3,2,1,0:T(8,128)(2,1)} %bitcast.1.q_ref.k_ref.v_ref, bf16[4,1,16,32,384]{4,3,2,1,0:T(8,128)(2,1)} %bitcast.1.q_ref.k_ref.v_ref), custom_call_target="tpu_custom_call" | custom-call | flops 943718400 | bytes 2097152 | tf_op jit(solution)/shard_map/pallas_call | solution.py:145
  123.9 2.0 %copy.7 = bf16[4,1,16,4,8,128]{5,4,2,3,0,1:T(8,128)(2,1)} copy(bf16[4,1,16,4,8,128]{5,4,3,2,0,1:T(8,128)(2,1)} %bitcast.32) | data formatting | bytes 1048576 | tf_op jit(solution)/shard_map/reshape | solution.py:261
  125.9 0.0 all-to-all-done.3
  125.9 6.0 %all-to-all-start.1 = ((bf16[16,128,128]{2,1,0:T(8,128)(2,1)}), bf16[16,128,128]{2,1,0:T(8,128)(2,1)S(1)}, u32[]{:S(2)}, u32[]{:S(2)}) async-start(bf16[16,128,128]{2,1,0:T(8,128)(2,1)} %bitcast.4), calls=%async_computation.1 | async-start | bytes 1048576 | tf_op jit(solution)/shard_map/all_to_all | solution.py:263
  132.0 1.1 copy.10
  133.1 13.2 %all-to-all-done.1 = bf16[16,128,128]{2,1,0:T(8,128)(2,1)S(1)} async-done(((bf16[16,128,128]{2,1,0:T(8,128)(2,1)}), bf16[16,128,128]{2,1,0:T(8,128)(2,1)S(1)}, u32[]{:S(2)}, u32[]{:S(2)}) %all-to-all-start.1) | async-done | bytes 524320 | tf_op jit(solution)/shard_map/all_to_all | solution.py:263
  146.2 1.1 copy.9
  147.3 2.4 %maximum_bitcast_fusion = bf16[4,8,16,4,1,2,1,128]{7,5,3,2,1,0,6,4:T(2,128)(2,1)S(1)} fusion(bf16[1,4,1,4,1,16,8,128]{7,0,1,5,6,3,2,4:T(2,128)(2,1)S(1)} %copy.10, bf16[1,4,1,4,1,16,8,128]{7,0,1,5,6,3,2,4:T(2,128)(2,1)S(1)} %copy.9), kind=kLoop, calls=%fused_computation.5 | loop fusion | flops 2097152 | bytes 2097152 | tf_op jit(solution)/shard_map/transpose | solution.py:266
  149.7 0.7 reshape.47
  150.5 0.1 dynamic-slice_bitcast_fusion.3
  150.5 0.3 multiply_reduce_fusion
  150.8 4.5 %multiply_convert_fusion = bf16[512,2048]{1,0:T(8,128)(2,1)S(1)} fusion(bf16[1024,2048]{1,0:T(8,128)(2,1)} %pad_maximum_fusion, f32[512]{0:T(512)S(1)} %add_rsqrt_fusion, bf16[512,256]{1,0:T(8,128)(2,1)S(1)} %get-tuple-element.10, bf16[512,256]{1,0:T(8,128)(2,1)S(1)} %get-tuple-element.11, bf16[512,256]{1,0:T(8,128)(2,1)S(1)} %get-tuple-element.12, ...), kind=kOutput, calls=%fused_computation.1 | convolution fusion | flops 2153775104 | bytes 7342080 | tf_op jit(solution)/shard_map/dot_general | solution.py:274
  155.4 2.2 %reshape.48 = bf16[128,4,2048]{2,1,0:T(4,128)(2,1)} reshape(bf16[512,2048]{1,0:T(8,128)(2,1)S(1)} %multiply_convert_fusion) | data formatting | bytes 4194304 | tf_op jit(solution)/shard_map/reshape | solution.py:275
  (2 shorter events, 0.0 us)
Async XLA Ops:
  13.5 6.5 %copy-start = (bf16[256,2048]{1,0:T(8,128)(2,1)S(1)}, bf16[256,2048]{1,0:T(8,128)(2,1)}, u32[]{:S(2)}) copy-start(bf16[256,2048]{1,0:T(8,128)(2,1)} %param.11) | copy-start | bytes 3145732
  13.5 6.5 %copy-start.1 = (f32[256]{0:T(256)S(1)}, f32[256]{0:T(256)}, u32[]{:S(2)}) copy-start(f32[256]{0:T(256)} %param.10) | copy-start | bytes 3076
  13.5 43.5 %all-to-all-start.2 = ((bf16[4,512,384]{2,1,0:T(8,128)(2,1)}), bf16[4,512,384]{2,1,0:T(8,128)(2,1)}, u32[]{:S(2)}, u32[]{:S(2)}) async-start(bf16[4,512,384]{2,1,0:T(8,128)(2,1)} %bitcast.28), calls=%async_computation.2 | async-start | bytes 3145728 | tf_op jit(solution)/shard_map/all_to_all | solution.py:252
  20.2 41.2 %collective-permute-start = (bf16[256,2048]{1,0:T(8,128)(2,1)S(1)}, bf16[256,2048]{1,0:T(8,128)(2,1)S(1)}, u32[]{:S(2)}, u32[]{:S(2)}) collective-permute-start(bf16[256,2048]{1,0:T(8,128)(2,1)S(1)} %multiply_convert_fusion.1), channel_id=1, source_target_pairs={{0,2},{1,3},{2,0},{3,1},{4,6},{5,7},{6,4},{7,5},{8,10},{9,11},{10,... | collective-permute-start | bytes 3145736 | tf_op jit(solution)/shard_map/ppermute | solution.py:232
  57.0 40.9 %all-to-all-start = ((bf16[4,512,384]{2,1,0:T(8,128)(2,1)}), bf16[4,512,384]{2,1,0:T(8,128)(2,1)}, u32[]{:S(2)}, u32[]{:S(2)}) async-start(bf16[4,512,384]{2,1,0:T(8,128)(2,1)} %bitcast.27), calls=%async_computation | async-start | bytes 3145728 | tf_op jit(solution)/shard_map/all_to_all | solution.py:252
  62.9 38.9 %collective-permute-start.1 = (bf16[512,2048]{1,0:T(8,128)(2,1)}, bf16[512,2048]{1,0:T(8,128)(2,1)}, u32[]{:S(2)}, u32[]{:S(2)}) collective-permute-start(bf16[512,2048]{1,0:T(8,128)(2,1)} %pad_maximum_fusion.1), channel_id=1, source_target_pairs={{0,1},{1,0},{2,3},{3,2},{4,5},{5,4},{6,7},{7,6},{8,9},{9,8},{10,11... | collective-permute-start | bytes 6291464 | tf_op jit(solution)/shard_map/ppermute | solution.py:232
  98.0 27.9 %all-to-all-start.3 = ((bf16[16,128,128]{2,1,0:T(8,128)(2,1)}), bf16[16,128,128]{2,1,0:T(8,128)(2,1)S(1)}, u32[]{:S(2)}, u32[]{:S(2)}) async-start(bf16[16,128,128]{2,1,0:T(8,128)(2,1)} %bitcast.10), calls=%async_computation.3 | async-start | bytes 1048576 | tf_op jit(solution)/shard_map/all_to_all | solution.py:263
  125.9 20.3 %all-to-all-start.1 = ((bf16[16,128,128]{2,1,0:T(8,128)(2,1)}), bf16[16,128,128]{2,1,0:T(8,128)(2,1)S(1)}, u32[]{:S(2)}, u32[]{:S(2)}) async-start(bf16[16,128,128]{2,1,0:T(8,128)(2,1)} %bitcast.4), calls=%async_computation.1 | async-start | bytes 1048576 | tf_op jit(solution)/shard_map/all_to_all | solution.py:263
